TPU v7x, 32 devices: a whole 2x2x4 slice. The times are simulated.
32 devices in a mesh: sp: 8 (over z, x), tp: 4 (over y, core).
Axes of the slice: x: 2, y: 2, z: 4, core: 2. Of those that a mesh axis runs over, the one named last changes fastest.
Arguments:
- tokens: bfloat16 [1024, 2048], P(('sp', 'tp')), may hold values from -6 to 6
- norm_gain: float32 [2048], replicated, may hold values from 0.1 to 1.9
- w_query: bfloat16 [2048, 512], P(None, 'tp'), may hold values from -0.125 to 0.125
- w_key: bfloat16 [2048, 512], P(None, 'tp'), may hold values from -0.125 to 0.125
- w_value: bfloat16 [2048, 512], P(None, 'tp'), may hold values from -0.125 to 0.125
- score_offset: float32 [8], P('tp'), may hold values from -13 to -3, as said below
- w_out: bfloat16 [512, 2048], P('tp'), may hold values from -0.25 to 0.25
Outputs:
- mixed: bfloat16 [1024, 2048], P(('sp', 'tp'))
Inputs may be any that keep to these rules, and one draw needn't show every extreme that they name: `score_offset`: one offset a head.
All inputs are finite; a program needn't handle non-finite values.
Results may differ from a plain program's by a relative error of at most 0.01.
Values may be sent and summed in bfloat16 or wider, within the bound.
A program may use at most 64 MiB of HBM per device.

v0:
```python
import jax
import jax.numpy as jnp
from jax import lax
from jax.sharding import PartitionSpec as P

HEAD_DIM = 64


RMS_EPS = 1e-06


def from_behind(array, axis, by):
    count = lax.axis_size(axis)
    pairs = [(i, i + by) for i in range(count) if 0 <= i + by < count]
    return lax.ppermute(array, axis, pairs)


def per_device(tokens, norm_gain, w_query, w_key, w_value, score_offset, w_out):
    groups = lax.axis_size("tp")
    tok_rows = tokens.shape[0] * groups
    head_width = w_query.shape[1]
    heads_dev = score_offset.shape[0]
    rows_f32 = lax.all_gather(tokens, "tp", axis=0, tiled=True).astype(jnp.float32)
    inv_rms = lax.rsqrt(jnp.mean(rows_f32 * rows_f32, axis=1, keepdims=True) + RMS_EPS)
    normed = (rows_f32 * inv_rms * norm_gain).astype(jnp.bfloat16)
    projected = jnp.concatenate(
        [
            jnp.dot(normed, w_query, preferred_element_type=jnp.float32),
            jnp.dot(normed, w_key, preferred_element_type=jnp.float32),
            jnp.dot(normed, w_value, preferred_element_type=jnp.float32),
        ],
        axis=1,
    ).astype(jnp.bfloat16)
    queries = projected[:, :head_width].reshape(tok_rows, heads_dev, HEAD_DIM)
    key_vals = jnp.stack(
        [projected[:, head_width : 2 * head_width], projected[:, 2 * head_width :]]
    )
    own_index = lax.axis_index("sp")
    shards = lax.axis_size("sp")
    query_pos = own_index * tok_rows + jnp.arange(tok_rows, dtype=jnp.int32)
    offsets = score_offset[:, None, None]

    def absorb(running, key_block, key_start):
        totals, log_kept = running
        key_rows = key_block.shape[1]
        key_part = key_block[0].reshape(key_rows, heads_dev, HEAD_DIM)
        value_part = key_block[1].reshape(key_rows, heads_dev, HEAD_DIM)
        key_pos = key_start + jnp.arange(key_rows, dtype=jnp.int32)
        scores = (
            jnp.einsum("qhd,khd->hqk", queries, key_part, preferred_element_type=jnp.float32)
            * HEAD_DIM ** (-0.5)
            + offsets
        )
        earlier = ((key_pos[None, :] < query_pos[:, None]) & (key_pos[None, :] >= 0))[None]
        log_keep = jnp.where(earlier, jax.nn.log_sigmoid(-scores), 0.0)
        suffix = lax.cumsum(log_keep, axis=2, reverse=True) - log_keep + log_kept[:, :, None]
        weights = jnp.where(earlier, jnp.exp(jax.nn.log_sigmoid(scores) + suffix), 0.0).astype(
            jnp.bfloat16
        )
        totals = totals + jnp.einsum(
            "hqk,khd->hqd", weights, value_part, preferred_element_type=jnp.float32
        )
        return (totals, log_kept + jnp.sum(log_keep, axis=2))

    start_state = (
        jnp.zeros((heads_dev, tok_rows, HEAD_DIM), jnp.float32),
        jnp.zeros((heads_dev, tok_rows), jnp.float32),
    )
    lower_one = from_behind(key_vals, "sp", 1)
    paired = jnp.concatenate([lower_one, key_vals], axis=1)
    lower_two = from_behind(paired, "sp", 2)
    four_spans = jnp.concatenate([lower_two, paired], axis=1)
    running = absorb(start_state, four_spans, (own_index - 3) * tok_rows)

    def regroup(turn_idx, packed):
        key_block, carried = packed
        key_block = from_behind(key_block, "sp", 4)
        return (key_block, absorb(carried, key_block, (own_index - 3 - 4 * turn_idx) * tok_rows))

    finished = lax.fori_loop(1, shards // 4, regroup, (four_spans, running))[1]
    mixed_rows = finished[0].transpose(1, 0, 2).reshape(tok_rows, head_width).astype(jnp.bfloat16)
    return lax.psum_scatter(
        jnp.dot(mixed_rows, w_out, preferred_element_type=jnp.float32).astype(jnp.bfloat16),
        "tp",
        scatter_dimension=0,
        tiled=True,
    )


def solution(mesh):
    return jax.shard_map(
        per_device,
        mesh=mesh,
        in_specs=(
            P(("sp", "tp"), None),
            P(),
            P(None, "tp"),
            P(None, "tp"),
            P(None, "tp"),
            P("tp"),
            P("tp", None),
        ),
        out_specs=P(("sp", "tp"), None),
        check_vma=False,
    )
```

profile of v0, /device:TPU:0, one launch (start us, length us, event | category | flops | bytes accessed | tf_op | source)
XLA Modules:
  0.0 83.2 jit_solution(1310046892703350980)
XLA Ops:
  6.5 0.0 copy-start
  6.5 0.0 copy-start.2
  6.5 0.0 reduce-scatter.2.cloned.1.call-start
  6.5 9.0 %all_gather.3 = bf16[128,2048]{1,0:T(8,128)(2,1)S(1)} all-gather(bf16[32,2048]{1,0:T(8,128)(2,1)} %param.7), channel_id=1, replica_groups=mesh['sp'=8,'tp'=4] {'tp'}, dimensions={0}, use_global_device_ids=true | all-gather | bytes 655360 | tf_op jit(solution)/shard_map/all_gather | solution.py:23
  15.5 0.0 copy-start.5
  15.5 0.2 fusion.13
  15.7 0.0 copy-done.2
  15.8 0.5 copy-done.5
  16.2 0.0 copy-start.3
  16.2 0.4 fusion.11
  16.6 0.7 copy-done.3
  17.3 0.0 copy-start.4
  17.3 0.4 fusion.12
  17.7 3.4 %collective-permute-start = (bf16[2,128,128]{2,1,0:T(8,128)(2,1)S(1)}, bf16[2,128,128]{2,1,0:T(8,128)(2,1)S(1)}, u32[]{:S(2)}, u32[]{:S(2)}) collective-permute-start(bf16[2,128,128]{2,1,0:T(8,128)(2,1)S(1)} %pad_maximum_fusion), channel_id=1, source_target_pairs={{0,4},{4,8},{8,12},{12,16},{16,20},{20,24},{24,28},{1,5},{5,9},{9,... | collective-permute-start | bytes 196616 | tf_op jit(solution)/shard_map/ppermute | solution.py:15
  21.1 0.0 copy-done.4
  21.1 0.4 convolution_convert_fusion.3
  21.5 1.4 %collective-permute-done = bf16[2,128,128]{2,1,0:T(8,128)(2,1)S(1)} collective-permute-done((bf16[2,128,128]{2,1,0:T(8,128)(2,1)S(1)}, bf16[2,128,128]{2,1,0:T(8,128)(2,1)S(1)}, u32[]{:S(2)}, u32[]{:S(2)}) %collective-permute-start) | collective-permute-done | bytes 65568 | tf_op jit(solution)/shard_map/ppermute | solution.py:15
  23.0 5.3 %collective-permute-start.1 = (bf16[2,256,128]{2,1,0:T(8,128)(2,1)S(1)}, bf16[2,256,128]{2,1,0:T(8,128)(2,1)S(1)}, u32[]{:S(2)}, u32[]{:S(2)}) collective-permute-start(bf16[2,256,128]{2,1,0:T(8,128)(2,1)S(1)} %maximum_maximum_fusion.1), channel_id=1, source_target_pairs={{0,8},{4,12},{8,16},{12,20},{16,24},{20,28},{1,9},{5,13},{9,17},{1... | collective-permute-start | bytes 393224 | tf_op jit(solution)/shard_map/ppermute | solution.py:15
  28.3 0.2 compare_and_fusion
  28.5 2.3 %collective-permute-done.1 = bf16[2,256,128]{2,1,0:T(8,128)(2,1)S(1)} collective-permute-done((bf16[2,256,128]{2,1,0:T(8,128)(2,1)S(1)}, bf16[2,256,128]{2,1,0:T(8,128)(2,1)S(1)}, u32[]{:S(2)}, u32[]{:S(2)}) %collective-permute-start.1) | collective-permute-done | bytes 131104 | tf_op jit(solution)/shard_map/ppermute | solution.py:15
  30.9 5.4 %collective-permute-start.2 = (bf16[2,512,128]{2,1,0:T(8,128)(2,1)S(1)}, bf16[2,512,128]{2,1,0:T(8,128)(2,1)S(1)}, u32[]{:S(2)}, u32[]{:S(2)}) collective-permute-start(bf16[2,512,128]{2,1,0:T(8,128)(2,1)S(1)} %maximum_maximum_fusion), channel_id=1, source_target_pairs={{0,16},{4,20},{8,24},{12,28},{1,17},{5,21},{9,25},{13,29},{2,18},{... | collective-permute-start | bytes 786440 | tf_op jit(solution)/shard_map/while/body/eval_jaxpr/ppermute | solution.py:15
  36.2 0.1 copy.16
  36.4 0.0 copy-start.1
  36.4 0.6 copy-done.1
  37.0 0.3 fusion.37
  37.3 0.4 negate_select_fusion
  37.7 0.2 reshape.141
  37.9 0.2 copy.17
  38.1 2.2 %fusion.47 = f32[2,128,4,128]{1,2,3,0:T(4,128)S(1)} fusion(f32[2,128,4,128]{1,2,3,0:T(4,128)S(1)} %copy.17), kind=kOutput, calls=%fused_computation.70 | output fusion | flops 16646144 | bytes 1048576 | tf_op jit(solution)/shard_map/reduce-window
  40.4 0.1 broadcast_add_fusion.1
  40.4 0.1 copy.19
  40.6 0.2 copy.18
  40.8 0.2 reduce_window_sum.26
  41.0 0.9 %fusion.35 = f32[2,128,64]{1,2,0:T(8,128)S(1)} fusion(bf16[512,2,64]{0,2,1:T(8,128)(2,1)S(1)} %bitcast.32, f32[2,128,512]{2,1,0:T(8,128)S(1)} %reduce_window_sum.26, f32[2,128,512]{2,1,0:T(8,128)S(1)} %get-tuple-element.38, pred[128,512]{1,0:T(8,128)(4,1)S(1)} %get-tuple-element.26, u8[128,512]{1,0:T(8,128)(4,1)S(1)} %get-tuple-element.36), kind=kOutput, calls=%fused_computation.53 | convolution fusion | flops 19791872 | bytes 1376256 | tf_op jit(solution)/shard_map/hqk,khd->hqd/dot_general | solution.py:60
  41.9 0.0 collective-permute-done.2
  41.9 0.1 copy.20
  42.1 0.1 copy.23
  42.2 1.3 %fusion.24 = (f32[2,128,512]{2,1,0:T(8,128)S(1)}, f32[2,128,512]{2,1,0:T(8,128)}) fusion(pred[128,512]{1,0:T(8,128)(4,1)S(1)} %get-tuple-element.25, f32[2]{0:T(128)S(1)} %copy-done.1, bf16[128,2,64]{0,2,1:T(8,128)(2,1)S(1)} %bitcast.34, bf16[512,2,64]{0,2,1:T(8,128)(2,1)S(1)} %bitcast.31), kind=kOutput, calls=%fused_computation.34 | convolution fusion | flops 18087936 | bytes 1277960 | tf_op jit(solution)/shard_map/while/body/eval_jaxpr/qhd,khd->hqk/dot_general | solution.py:50
  43.5 0.2 reshape.143
  43.7 0.2 copy.21
  43.9 2.2 %fusion.48 = f32[2,128,4,128]{1,2,3,0:T(4,128)S(1)} fusion(f32[2,128,4,128]{1,2,3,0:T(4,128)S(1)} %copy.21), kind=kOutput, calls=%fused_computation.71 | output fusion | flops 16646144 | bytes 1048576 | tf_op jit(solution)/shard_map/reduce-window.2
  46.2 0.1 broadcast_add_fusion
  46.3 0.2 copy.22
  46.5 0.0 copy-start.6
  46.5 0.2 reduce_window_sum.28
  46.7 0.8 copy-done.6
  47.5 1.3 %fusion.10 = bf16[2,128,64]{1,2,0:T(8,128)(2,1)S(1)} fusion(f32[2,128,64]{1,2,0:T(8,128)S(1)} %fusion.35, bf16[512,2,64]{0,2,1:T(8,128)(2,1)S(1)} %bitcast.30, f32[2,128,512]{2,1,0:T(8,128)S(1)} %reduce_window_sum.28, f32[2,128,512]{2,1,0:T(8,128)S(1)} %copy-done.6, pred[128,512]{1,0:T(8,128)(4,1)S(1)} %get-tuple-element.25, ...), kind=kOutput, calls=%fused_computation.18 | convolution fusion | flops 21005056 | bytes 1998848 | tf_op jit(solution)/shard_map/while/body/eval_jaxpr/hqk,khd->hqd/dot_general | solution.py:60
  48.9 0.0 copy-done
  48.9 1.1 %convolution_convert_fusion = bf16[128,2048]{1,0:T(8,128)(2,1)} fusion(bf16[128,128]{0,1:T(8,128)(2,1)S(1)} %bitcast.35, bf16[128,2048]{1,0:T(8,128)(2,1)S(1)} %copy-done), kind=kOutput, calls=%fused_computation.1 | convolution fusion | flops 67371008 | bytes 1081344 | tf_op jit(solution)/shard_map/dot_general | solution.py:83
  50.0 0.0 reduce-scatter.2.cloned.1.call-update
  50.0 26.4 %reduce-scatter.2.cloned.1.call-done = bf16[32,2048]{1,0:T(8,128)(2,1)} async-done(((bf16[128,2048]{1,0:T(8,128)(2,1)}), bf16[32,2048]{1,0:T(8,128)(2,1)}) %reduce-scatter.2.cloned.1.call-update) | async-done | bytes 131088 | tf_op jit(solution)/shard_map/reduce_scatter | solution.py:82
  (15 shorter events, 0.2 us)
Async XLA Ops:
  6.5 42.3 %copy-start = (bf16[128,2048]{1,0:T(8,128)(2,1)S(1)}, bf16[128,2048]{1,0:T(8,128)(2,1)}, u32[]{:S(2)}) copy-start(bf16[128,2048]{1,0:T(8,128)(2,1)} %param.13) | copy-start | bytes 1572868
  6.5 9.2 %copy-start.2 = (bf16[2048,128]{1,0:T(8,128)(2,1)S(1)}, bf16[2048,128]{1,0:T(8,128)(2,1)}, u32[]{:S(2)}) copy-start(bf16[2048,128]{1,0:T(8,128)(2,1)} %param.10) | copy-start | bytes 1572868
  6.5 69.9 %reduce-scatter.2.cloned.1.call-start = ((), (), s32[]{:S(2)}) async-start(), calls=%async_computation.1 | async-start | bytes 655360 | tf_op jit(solution)/shard_map/reduce_scatter | solution.py:82
  15.5 0.7 copy-start.5
  16.2 1.0 %copy-start.3 = (bf16[2048,128]{1,0:T(8,128)(2,1)S(1)}, bf16[2048,128]{1,0:T(8,128)(2,1)}, u32[]{:S(2)}) copy-start(bf16[2048,128]{1,0:T(8,128)(2,1)} %param.11) | copy-start | bytes 1572868
  17.3 3.8 %copy-start.4 = (bf16[2048,128]{1,0:T(8,128)(2,1)S(1)}, bf16[2048,128]{1,0:T(8,128)(2,1)}, u32[]{:S(2)}) copy-start(bf16[2048,128]{1,0:T(8,128)(2,1)} %param.9) | copy-start | bytes 1572868
  17.7 5.3 %collective-permute-start = (bf16[2,128,128]{2,1,0:T(8,128)(2,1)S(1)}, bf16[2,128,128]{2,1,0:T(8,128)(2,1)S(1)}, u32[]{:S(2)}, u32[]{:S(2)}) collective-permute-start(bf16[2,128,128]{2,1,0:T(8,128)(2,1)S(1)} %pad_maximum_fusion), channel_id=1, source_target_pairs={{0,4},{4,8},{8,12},{12,16},{16,20},{20,24},{24,28},{1,5},{5,9},{9,... | collective-permute-start | bytes 196616 | tf_op jit(solution)/shard_map/ppermute | solution.py:15
  23.0 7.8 %collective-permute-start.1 = (bf16[2,256,128]{2,1,0:T(8,128)(2,1)S(1)}, bf16[2,256,128]{2,1,0:T(8,128)(2,1)S(1)}, u32[]{:S(2)}, u32[]{:S(2)}) collective-permute-start(bf16[2,256,128]{2,1,0:T(8,128)(2,1)S(1)} %maximum_maximum_fusion.1), channel_id=1, source_target_pairs={{0,8},{4,12},{8,16},{12,20},{16,24},{20,28},{1,9},{5,13},{9,17},{1... | collective-permute-start | bytes 393224 | tf_op jit(solution)/shard_map/ppermute | solution.py:15
  30.9 11.0 %collective-permute-start.2 = (bf16[2,512,128]{2,1,0:T(8,128)(2,1)S(1)}, bf16[2,512,128]{2,1,0:T(8,128)(2,1)S(1)}, u32[]{:S(2)}, u32[]{:S(2)}) collective-permute-start(bf16[2,512,128]{2,1,0:T(8,128)(2,1)S(1)} %maximum_maximum_fusion), channel_id=1, source_target_pairs={{0,16},{4,20},{8,24},{12,28},{1,17},{5,21},{9,25},{13,29},{2,18},{... | collective-permute-start | bytes 786440 | tf_op jit(solution)/shard_map/while/body/eval_jaxpr/ppermute | solution.py:15
  36.4 0.7 copy-start.1
  46.5 1.0 %copy-start.6 = (f32[2,128,512]{2,1,0:T(8,128)S(1)}, f32[2,128,512]{2,1,0:T(8,128)}, u32[]{:S(2)}) copy-start(f32[2,128,512]{2,1,0:T(8,128)} %get-tuple-element.41) | copy-start | bytes 1572868
Sparse Core Ops, SparseCore 0:
  50.1 26.2 reduce-scatter.1
where the time goes:
time: 83.6 us; the launch traced here: 83.2 us
  waiting for transfers between devices  30.2 us (36%)
  starting transfers between devices  14.1 us (17%)
  between operations  13.7 us (16%)
  blocking collectives  9 us (11%)
  matrix products  6.06 us (7%)
  other arithmetic  5.33 us (6%)
  local copies, waits for them, and re-layouts  4.88 us (6%)
    reduce_scatter x1, waiting for transfers between devices, per_device(): lax.psum_scatter(jnp.dot(mixed_rows, w_out, preferred_element_type=jnp.fl...  26.4 us
    ppermute x3, starting transfers between devices, from_behind(): return lax.ppermute(array, axis, pairs)  14.1 us
    all_gather x1, blocking collectives, per_device(): lax.all_gather(tokens, 'tp', axis=0, tiled=True).astype(jnp.float32)  9 us
    another operation x4, other arithmetic  4.37 us
    ppermute x3, waiting for transfers between devices, from_behind(): return lax.ppermute(array, axis, pairs)  3.76 us
    unnamed x14, local copies, waits for them, and re-layouts  2.66 us
    dot_general x2, matrix products, absorb(): jnp.einsum('hqk,khd->hqd', weights, value_part, preferred_element_type=jn...  2.19 us
  transfers between devices with their start and end apart: 4, of which 3 were waited for; matrix products, arithmetic and copies ran while one was open for 7% of the time, Pallas kernels for 0%

commit v1 on v0

v1 whole, which is shorter than its diff:
```python
import functools

import jax
import jax.numpy as jnp
from jax import lax
from jax.experimental import pallas as pl
from jax.experimental.pallas import tpu as pltpu
from jax.sharding import PartitionSpec as P

HEAD_DIM = 64
RMS_EPS = 1e-06
MESH = pl.DeviceIdType.MESH
F32 = jnp.float32
BF16 = jnp.bfloat16


def layer_kernel(
    n_sp,
    n_tp,
    lanes,
    tok_ref,
    gain_ref,
    wq_ref,
    wk_ref,
    wv_ref,
    off_ref,
    wout_ref,
    out_ref,
    tok_buf,
    w_buf,
    wo_buf,
    normed,
    kv_out,
    q_out,
    kv_buf,
    q_buf,
    att_out,
    att_buf,
    load_sem,
    tok_send,
    tok_recv,
    wo_send,
    wo_recv,
    kv_send,
    kv_recv,
    q_send,
    q_recv,
    att_send,
    att_recv,
):
    s = lax.axis_index("sp")
    t = lax.axis_index("tp")
    heads = kv_out.shape[0]
    rows = kv_out.shape[1]
    piece = tok_buf.shape[1]
    width = 2 * HEAD_DIM
    groups = n_sp // heads
    a = s // heads
    b = s % heads
    pair_hi = t // lanes
    pair_lo = t % lanes
    n_hi = n_tp // lanes

    loads = [
        pltpu.make_async_copy(tok_ref, tok_buf.at[t], load_sem.at[0]),
        pltpu.make_async_copy(wq_ref, w_buf.at[:, pl.ds(0, width)], load_sem.at[1]),
        pltpu.make_async_copy(wk_ref, w_buf.at[:, pl.ds(width, width)], load_sem.at[2]),
        pltpu.make_async_copy(wv_ref, w_buf.at[:, pl.ds(2 * width, width)], load_sem.at[3]),
        pltpu.make_async_copy(wout_ref, wo_buf.at[t], load_sem.at[4]),
    ]
    for load in loads:
        load.start()

    barrier = pltpu.get_barrier_semaphore()
    for i in range(1, n_tp):
        other = (t + i) % n_tp
        for j in range(heads):
            peer = a * heads + (b + j) % heads
            pl.semaphore_signal(barrier, inc=1, device_id=(peer, other), device_id_type=MESH)

    def greet(i, carry):
        pl.semaphore_signal(barrier, inc=1, device_id=((s + i) % n_sp, t), device_id_type=MESH)
        return carry

    lax.fori_loop(1, n_sp, greet, 0)
    pl.semaphore_wait(barrier, (n_tp - 1) * heads + n_sp - 1)

    def send(src, dst, send_sem, recv_sem, device):
        return pltpu.make_async_remote_copy(
            src_ref=src,
            dst_ref=dst,
            send_sem=send_sem,
            recv_sem=recv_sem,
            device_id=device,
            device_id_type=MESH,
        )

    def gather(buf, send_sems, recv_sems):
        sends = []
        for i in range(1, n_hi):
            dest = (pair_hi + i) % n_hi * lanes + pair_lo
            sends.append(send(buf.at[t], buf.at[t], send_sems.at[i * lanes], recv_sems.at[t], (s, dest)))
        for j in range(1, lanes):
            dest = pair_hi * lanes + (pair_lo + j) % lanes
            sends.append(send(buf.at[t], buf.at[t], send_sems.at[j], recv_sems.at[t], (s, dest)))
        return sends

    def arrival(buf, recv_sems, source):
        pltpu.make_async_copy(buf.at[source], buf.at[source], recv_sems.at[source]).wait()

    def relays(buf, send_sems, recv_sems, i, source):
        out = []
        for j in range(1, lanes):
            dest = pair_hi * lanes + (pair_lo + j) % lanes
            out.append(
                send(buf.at[source], buf.at[source], send_sems.at[i * lanes + j], recv_sems.at[source], (s, dest))
            )
        return out

    gain = gain_ref[...]

    def norm(source):
        x = tok_buf[source].astype(F32)
        inv = lax.rsqrt(jnp.mean(x * x, axis=1, keepdims=True) + RMS_EPS)
        normed[pl.ds(pl.multiple_of(source * piece, piece), piece), :] = (x * inv * gain).astype(BF16)

    loads[0].wait()
    pending = gather(tok_buf, tok_send, tok_recv)
    for copy in pending:
        copy.start()
    norm(t)
    for j in range(1, lanes):
        source = pair_hi * lanes + (pair_lo + j) % lanes
        arrival(tok_buf, tok_recv, source)
        norm(source)
    for i in range(1, n_hi):
        source = (pair_hi + i) % n_hi * lanes + pair_lo
        arrival(tok_buf, tok_recv, source)
        for copy in relays(tok_buf, tok_send, tok_recv, i, source):
            copy.start()
            pending.append(copy)
        norm(source)
    loads[4].wait()
    wo_pending = gather(wo_buf, wo_send, wo_recv)
    for copy in wo_pending:
        copy.start()
    for i in range(1, n_hi):
        for j in range(1, lanes):
            source = (pair_hi + i) % n_hi * lanes + (pair_lo + j) % lanes
            arrival(tok_buf, tok_recv, source)
            norm(source)
    for load in loads[1:4]:
        load.wait()

    projected = jnp.dot(normed[...], w_buf[...], preferred_element_type=F32).astype(BF16)
    blank = jnp.zeros((rows, HEAD_DIM), BF16)
    for h in range(heads):
        cols = slice(h * HEAD_DIM, (h + 1) * HEAD_DIM)
        keys = projected[:, width:][:, cols]
        vals = projected[:, 2 * width :][:, cols]
        kv_out[h] = jnp.concatenate([keys, vals], axis=1)
        q_out[h] = jnp.concatenate([projected[:, cols] * jnp.asarray(HEAD_DIM**-0.5, BF16), blank], axis=1)

    mine = pl.ds(pl.multiple_of(b * rows, rows), rows)
    kv_sends = []
    for j in range(1, heads):
        h = (b + j) % heads
        dest = (a * heads + h, t)
        kv_sends.append(send(q_out.at[h], q_buf.at[mine], q_send.at[j], q_recv.at[b], dest))
        kv_sends.append(send(kv_out.at[h], kv_buf.at[a, mine], kv_send.at[0, j], kv_recv.at[s], dest))
    for copy in kv_sends:
        copy.start()

    def kv_copy(k, j):
        h = (b + j) % heads
        return send(kv_out.at[h], kv_buf.at[a, mine], kv_send.at[k, j], kv_recv.at[s], ((a + k) * heads + h, t))

    later = groups - 1 - a

    def kv_start(i, carry):
        for j in range(heads):
            kv_copy(later - i, j).start()
        return carry

    lax.fori_loop(0, later, kv_start, 0)
    kv_buf[a, mine, :] = kv_out[b]
    q_buf[mine, :] = q_out[b]

    for j in range(1, heads):
        peer = (b + j) % heads
        spot = pl.ds(pl.multiple_of(peer * rows, rows), rows)
        pltpu.make_async_copy(q_buf.at[spot], q_buf.at[spot], q_recv.at[peer]).wait()

    span = heads * rows
    offset = off_ref[b]
    row_id = lax.broadcasted_iota(jnp.int32, (span, span), 0)
    col_id = lax.broadcasted_iota(jnp.int32, (span, span), 1)
    below = row_id > col_id
    tri = jnp.where(below, 1.0, 0.0).astype(BF16)
    queries = q_buf[...]

    def block(group, masked, total, kept):
        kv = kv_buf[group]
        z = lax.dot_general(queries, kv, (((1,), (1,)), ((), ())), preferred_element_type=F32) + offset
        log_keep = -(jnp.maximum(z, 0.0) + jnp.log1p(jnp.exp(-jnp.abs(z))))
        log_take = z + log_keep
        if masked:
            log_keep = jnp.where(below, log_keep, 0.0)
        high = log_keep.astype(BF16)
        low = (log_keep - high.astype(F32)).astype(BF16)
        suffix = jnp.dot(high, tri, preferred_element_type=F32) + jnp.dot(low, tri, preferred_element_type=F32)
        weights = jnp.exp(log_take + suffix + kept)
        if masked:
            weights = jnp.where(below, weights, 0.0)
        total = total + jnp.dot(weights.astype(BF16), kv, preferred_element_type=F32)
        return total, kept + suffix[:, :1] + log_keep[:, :1]

    def kv_arrival(group, peer):
        spot = kv_buf.at[group, pl.ds(pl.multiple_of(peer * rows, rows), rows)]
        pltpu.make_async_copy(spot, spot, kv_recv.at[group * heads + peer]).wait()

    for j in range(1, heads):
        kv_arrival(a, (b + j) % heads)
    total, kept = block(a, True, jnp.zeros((span, width), F32), jnp.zeros((span, 1), F32))

    def absorb(i, carry):
        group = a - 1 - i
        for peer in range(heads):
            kv_arrival(group, peer)
        return block(group, False, *carry)

    total, kept = lax.fori_loop(0, a, absorb, (total, kept))

    att_out[...] = total.astype(BF16).reshape(att_out.shape)
    att_sends = []
    for j in range(heads):
        for i in range(n_tp):
            if i == 0 and j == 0:
                continue
            peer = (b + j) % heads
            other = (t + i) % n_tp
            att_sends.append(
                send(
                    att_out.at[peer * n_tp + other],
                    att_buf.at[t * heads + b],
                    att_send.at[j * n_tp + i],
                    att_recv.at[t * heads + b],
                    (a * heads + peer, other),
                )
            )
    for copy in att_sends:
        copy.start()
    att_buf[t * heads + b] = att_out[b * n_tp + t]

    for i in range(1, n_hi):
        source = (pair_hi + i) % n_hi * lanes + pair_lo
        arrival(wo_buf, wo_recv, source)
        for copy in relays(wo_buf, wo_send, wo_recv, i, source):
            copy.start()
            wo_pending.append(copy)
    for j in range(heads):
        for i in range(n_tp):
            if i or j:
                arrival(att_buf, att_recv, (t + i) % n_tp * heads + (b + j) % heads)

    def partial(source):
        parts = [att_buf[source * heads + h][:, HEAD_DIM:] for h in range(heads)]
        part = jnp.dot(jnp.concatenate(parts, axis=1), wo_buf[source], preferred_element_type=F32)
        return part.astype(BF16).astype(F32)

    mixed = partial(t)
    for j in range(1, lanes):
        source = pair_hi * lanes + (pair_lo + j) % lanes
        arrival(wo_buf, wo_recv, source)
        mixed = mixed + partial(source)
    for i in range(1, n_hi):
        mixed = mixed + partial((pair_hi + i) % n_hi * lanes + pair_lo)
    for i in range(1, n_hi):
        for j in range(1, lanes):
            source = (pair_hi + i) % n_hi * lanes + (pair_lo + j) % lanes
            arrival(wo_buf, wo_recv, source)
            mixed = mixed + partial(source)
    out_ref[...] = mixed.astype(BF16)

    for copy in pending + wo_pending + kv_sends + att_sends:
        copy.wait_send()

    def kv_done(i, carry):
        for j in range(heads):
            kv_copy(later - i, j).wait_send()
        return carry

    lax.fori_loop(0, later, kv_done, 0)


def per_device(tokens, norm_gain, w_query, w_key, w_value, score_offset, w_out):
    n_tp = lax.axis_size("tp")
    n_sp = lax.axis_size("sp")
    piece, model = tokens.shape
    width = w_query.shape[1]
    heads = score_offset.shape[0]
    rows = piece * n_tp
    lanes = 2 if n_tp % 2 == 0 else 1
    groups = n_sp // heads
    lane_width = 2 * HEAD_DIM
    dma = pltpu.SemaphoreType.DMA
    anywhere = pl.BlockSpec(memory_space=pl.ANY)
    vmem = pl.BlockSpec(memory_space=pltpu.VMEM)
    return pl.pallas_call(
        functools.partial(layer_kernel, n_sp, n_tp, lanes),
        out_shape=jax.ShapeDtypeStruct((piece, w_out.shape[1]), BF16),
        in_specs=[
            anywhere,
            vmem,
            anywhere,
            anywhere,
            anywhere,
            pl.BlockSpec(memory_space=pltpu.SMEM),
            anywhere,
        ],
        out_specs=vmem,
        scratch_shapes=[
            pltpu.VMEM((n_tp, piece, model), BF16),
            pltpu.VMEM((model, 3 * width), BF16),
            pltpu.VMEM((n_tp, width, w_out.shape[1]), BF16),
            pltpu.VMEM((rows, model), BF16),
            pltpu.VMEM((heads, rows, lane_width), BF16),
            pltpu.VMEM((heads, rows, lane_width), BF16),
            pltpu.VMEM((groups, heads * rows, lane_width), BF16),
            pltpu.VMEM((heads * rows, lane_width), BF16),
            pltpu.VMEM((heads * n_tp, piece, lane_width), BF16),
            pltpu.VMEM((heads * n_tp, piece, lane_width), BF16),
            dma((5,)),
            dma((n_tp,)),
            dma((n_tp,)),
            dma((n_tp,)),
            dma((n_tp,)),
            dma((groups, heads)),
            dma((n_sp,)),
            dma((heads,)),
            dma((heads,)),
            dma((heads * n_tp,)),
            dma((heads * n_tp,)),
        ],
        compiler_params=pltpu.CompilerParams(collective_id=0, has_side_effects=True),
    )(tokens, norm_gain.reshape(1, model), w_query, w_key, w_value, score_offset, w_out)


def solution(mesh):
    return jax.shard_map(
        per_device,
        mesh=mesh,
        in_specs=(
            P(("sp", "tp"), None),
            P(),
            P(None, "tp"),
            P(None, "tp"),
            P(None, "tp"),
            P("tp"),
            P("tp", None),
        ),
        out_specs=P(("sp", "tp"), None),
        check_vma=False,
    )
```

time: 83.6 us -> 28.5 us (0.34)
  waiting for transfers between devices: 30.2 us -> 0 us
  Pallas kernels: 0 us -> 26.6 us
  starting transfers between devices: 14.1 us -> 0 us
  between operations: 13.7 us -> 0.01 us
  blocking collectives: 9 us -> 0 us
  matrix products: 6.06 us -> 0 us
  other arithmetic: 5.33 us -> 0 us
  local copies, waits for them, and re-layouts: 4.88 us -> 1.57 us
    pallas_call x0 -> x1, Pallas kernels: none -> 26.6 us  [per_device(): pl.pallas_call(functools.partial(layer_kernel, n_sp, n_tp, lanes), out_sh...]
    reduce_scatter x1 -> x0, waiting for transfers between devices: 26.4 us -> none  [per_device(): lax.psum_scatter(jnp.dot(mixed_rows, w_out, preferred_element_type=jnp.fl...]
    ppermute x3 -> x0, starting transfers between devices: 14.1 us -> none  [from_behind(): return lax.ppermute(array, axis, pairs)]
    all_gather x1 -> x0, blocking collectives: 9 us -> none  [per_device(): lax.all_gather(tokens, 'tp', axis=0, tiled=True).astype(jnp.float32)]
    dot_general x8 -> x0, matrix products: 6.06 us -> none  [the longest x2 2.19 us: absorb(): jnp.einsum('hqk,khd->hqd', weights, value_part, preferred_element_type=jn...]
    another operation x7 -> x0, other arithmetic: 4.57 us -> none
    ppermute x3 -> x0, waiting for transfers between devices: 3.76 us -> none  [from_behind(): return lax.ppermute(array, axis, pairs)]
    another operation x10 -> x0, local copies, waits for them, and re-layouts: 1.32 us -> none  [the longest x4 0.89 us: absorb(): lax.cumsum(log_keep, axis=2, reverse=True) - log_keep + log_kept[:, :, None]]
  transfers between devices with their start and end apart: 4 -> 0, of which waited for: 3 -> 0; matrix products, arithmetic and copies ran while one was open for 7% -> 0% of each run, Pallas kernels for 0% -> 0%
where the time goes in v1:
time: 28.5 us; the launch traced here: 28.2 us
  Pallas kernels  26.6 us (93%)
  local copies, waits for them, and re-layouts  1.57 us (6%)
    pallas_call x1, Pallas kernels, per_device(): pl.pallas_call(functools.partial(layer_kernel, n_sp, n_tp, lanes), out_sh...  26.6 us
    unnamed x1, local copies, waits for them, and re-layouts  1.57 us

profile of v1, /device:TPU:0, one launch (start us, length us, event | category | flops | bytes accessed | tf_op | source)
XLA Modules:
  0.0 28.2 jit_solution(2610100660942445228)
XLA Ops:
  0.0 26.6 %shard_map.73 = bf16[32,2048]{1,0:T(8,128)(2,1)} custom-call(bf16[32,2048]{1,0:T(8,128)(2,1)} %tok_ref.1, f32[1,2048]{1,0:T(1,128)} %bitcast.1, bf16[2048,128]{1,0:T(8,128)(2,1)} %wq_ref.1, bf16[2048,128]{1,0:T(8,128)(2,1)} %wk_ref.1, bf16[2048,128]{1,0:T(8,128)(2,1)} %wv_ref.1, f32[2]{0:T(128)} %off_ref.1, bf16[128,2048]{1,0:T(8,128)(2,1)} %wout_ref.1), custom_call_target="tpu_custom_call" | custom-call | tf_op jit(solution)/shard_map/pallas_call | solution.py:309
  26.6 1.6 %copy.9 = bf16[32,2048]{1,0:T(8,128)(2,1)} copy(bf16[32,2048]{1,0:T(8,128)(2,1)} %shard_map.73) | data formatting | bytes 262144

commit v2 on v1

--- a/solution.py
+++ b/solution.py
@@ -12,6 +12,7 @@
 MESH = pl.DeviceIdType.MESH
 F32 = jnp.float32
 BF16 = jnp.bfloat16
+PIECES = 4
 
 
 def layer_kernel(
@@ -36,6 +37,8 @@
     q_buf,
     att_out,
     att_buf,
+    chain_sem,
+    pair_sem,
     load_sem,
     tok_send,
     tok_recv,
@@ -73,17 +76,22 @@
 
     barrier = pltpu.get_barrier_semaphore()
     for i in range(1, n_tp):
-        other = (t + i) % n_tp
-        for j in range(heads):
-            peer = a * heads + (b + j) % heads
-            pl.semaphore_signal(barrier, inc=1, device_id=(peer, other), device_id_type=MESH)
-
-    def greet(i, carry):
-        pl.semaphore_signal(barrier, inc=1, device_id=((s + i) % n_sp, t), device_id_type=MESH)
-        return carry
-
-    lax.fori_loop(1, n_sp, greet, 0)
-    pl.semaphore_wait(barrier, (n_tp - 1) * heads + n_sp - 1)
+        pl.semaphore_signal(barrier, inc=1, device_id=(s, (t + i) % n_tp), device_id_type=MESH)
+    for j in range(1, heads):
+        pl.semaphore_signal(barrier, inc=1, device_id=(a * heads + (b + j) % heads, t), device_id_type=MESH)
+    has_next = a < groups - 1
+    has_prev = a > 0
+
+    @pl.when(has_next)
+    def _():
+        pl.semaphore_signal(barrier, inc=1, device_id=(s + heads, t), device_id_type=MESH)
+
+    @pl.when(has_prev)
+    def _():
+        pl.semaphore_signal(barrier, inc=1, device_id=(s - heads, t), device_id_type=MESH)
+
+    along = jnp.minimum(a, 1) + jnp.minimum(groups - 1 - a, 1)
+    pl.semaphore_wait(barrier, n_tp - 1 + heads - 1 + along)
 
     def send(src, dst, send_sem, recv_sem, device):
         return pltpu.make_async_remote_copy(
@@ -117,6 +125,31 @@
             )
         return out
 
+    wo_rows = wo_buf.shape[1] // PIECES
+
+    class wo_piece:
+        def __init__(self, c):
+            self.rows = pl.ds(c * wo_rows, wo_rows)
+
+        @property
+        def at(self):
+            return self
+
+        def __getitem__(self, source):
+            return wo_buf.at[source, self.rows]
+
+    def wo_relay(c):
+        for i in range(1, n_hi):
+            source = (pair_hi + i) % n_hi * lanes + pair_lo
+            arrival(wo_piece(c), wo_recv.at[c], source)
+            for copy in relays(wo_piece(c), wo_send.at[c], wo_recv.at[c], i, source):
+                copy.start()
+                wo_pending.append(copy)
+
+    def wo_arrival(source):
+        for c in range(PIECES):
+            arrival(wo_piece(c), wo_recv.at[c], source)
+
     gain = gain_ref[...]
 
     def norm(source):
@@ -128,6 +161,24 @@
     pending = gather(tok_buf, tok_send, tok_recv)
     for copy in pending:
         copy.start()
+
+    loads[4].wait()
+    wo_pending = []
+    for c in range(PIECES):
+        for copy in gather(wo_piece(c), wo_send.at[c], wo_recv.at[c]):
+            copy.start()
+            wo_pending.append(copy)
+
+    @pl.when(has_next)
+    def _():
+        pl.semaphore_wait(chain_sem, 1)
+
+    @pl.when(has_prev)
+    def _():
+        pl.semaphore_signal(chain_sem, inc=1, device_id=(s - heads, t), device_id_type=MESH)
+
+    for j in range(1, heads):
+        pl.semaphore_signal(pair_sem, inc=1, device_id=(a * heads + (b + j) % heads, t), device_id_type=MESH)
     norm(t)
     for j in range(1, lanes):
         source = pair_hi * lanes + (pair_lo + j) % lanes
@@ -140,10 +191,7 @@
             copy.start()
             pending.append(copy)
         norm(source)
-    loads[4].wait()
-    wo_pending = gather(wo_buf, wo_send, wo_recv)
-    for copy in wo_pending:
-        copy.start()
+    pl.semaphore_wait(pair_sem, heads - 1)
     for i in range(1, n_hi):
         for j in range(1, lanes):
             source = (pair_hi + i) % n_hi * lanes + (pair_lo + j) % lanes
@@ -222,6 +270,8 @@
     for j in range(1, heads):
         kv_arrival(a, (b + j) % heads)
     total, kept = block(a, True, jnp.zeros((span, width), F32), jnp.zeros((span, 1), F32))
+
+    wo_relay(0)
 
     def absorb(i, carry):
         group = a - 1 - i
@@ -252,12 +302,8 @@
         copy.start()
     att_buf[t * heads + b] = att_out[b * n_tp + t]
 
-    for i in range(1, n_hi):
-        source = (pair_hi + i) % n_hi * lanes + pair_lo
-        arrival(wo_buf, wo_recv, source)
-        for copy in relays(wo_buf, wo_send, wo_recv, i, source):
-            copy.start()
-            wo_pending.append(copy)
+    wo_relay(1)
+    wo_relay(2)
     for j in range(heads):
         for i in range(n_tp):
             if i or j:
@@ -271,14 +317,16 @@
     mixed = partial(t)
     for j in range(1, lanes):
         source = pair_hi * lanes + (pair_lo + j) % lanes
-        arrival(wo_buf, wo_recv, source)
+        wo_arrival(source)
         mixed = mixed + partial(source)
+    for c in range(3, PIECES):
+        wo_relay(c)
     for i in range(1, n_hi):
         mixed = mixed + partial((pair_hi + i) % n_hi * lanes + pair_lo)
     for i in range(1, n_hi):
         for j in range(1, lanes):
             source = (pair_hi + i) % n_hi * lanes + (pair_lo + j) % lanes
-            arrival(wo_buf, wo_recv, source)
+            wo_arrival(source)
             mixed = mixed + partial(source)
     out_ref[...] = mixed.astype(BF16)
 
@@ -308,7 +356,7 @@
     vmem = pl.BlockSpec(memory_space=pltpu.VMEM)
     return pl.pallas_call(
         functools.partial(layer_kernel, n_sp, n_tp, lanes),
-        out_shape=jax.ShapeDtypeStruct((piece, w_out.shape[1]), BF16),
+        out_shape=pltpu.VMEM((piece, w_out.shape[1]), BF16),
         in_specs=[
             anywhere,
             vmem,
@@ -330,11 +378,13 @@
             pltpu.VMEM((heads * rows, lane_width), BF16),
             pltpu.VMEM((heads * n_tp, piece, lane_width), BF16),
             pltpu.VMEM((heads * n_tp, piece, lane_width), BF16),
+            pltpu.SemaphoreType.REGULAR,
+            pltpu.SemaphoreType.REGULAR,
             dma((5,)),
             dma((n_tp,)),
             dma((n_tp,)),
-            dma((n_tp,)),
-            dma((n_tp,)),
+            dma((PIECES, n_tp)),
+            dma((PIECES, n_tp)),
             dma((groups, heads)),
             dma((n_sp,)),
             dma((heads,)),

time: 28.5 us -> 25.1 us (0.88)
  the two profiles are of different devices: /device:TPU:0 before, /device:TPU:21 now
where the time goes in v2:
time: 25.1 us; the launch traced here: 24.9 us
  Pallas kernels  24.2 us (96%)
  local copies, waits for them, and re-layouts  0.66 us (3%)
    pallas_call x1, Pallas kernels, per_device(): pl.pallas_call(functools.partial(layer_kernel, n_sp, n_tp, lanes), out_sh...  24.2 us
    unnamed x1, local copies, waits for them, and re-layouts  0.66 us

profile of v2, /device:TPU:21, one launch (start us, length us, event | category | flops | bytes accessed | tf_op | source)
XLA Modules:
  0.0 24.9 jit_solution(6004294975023710431)
XLA Ops:
  0.0 24.2 %shard_map.73 = bf16[32,2048]{1,0:T(8,128)(2,1)S(1)} custom-call(bf16[32,2048]{1,0:T(8,128)(2,1)} %tok_ref.1, f32[1,2048]{1,0:T(1,128)} %bitcast.1, bf16[2048,128]{1,0:T(8,128)(2,1)} %wq_ref.1, bf16[2048,128]{1,0:T(8,128)(2,1)} %wk_ref.1, bf16[2048,128]{1,0:T(8,128)(2,1)} %wv_ref.1, f32[2]{0:T(128)} %off_ref.1, bf16[128,2048]{1,0:T(8,128)(2,1)} %wout_ref.1), custom_call_target="tpu_custom_call" | custom-call | tf_op jit(solution)/shard_map/pallas_call | solution.py:357
  24.2 0.7 %copy.9 = bf16[32,2048]{1,0:T(8,128)(2,1)} copy(bf16[32,2048]{1,0:T(8,128)(2,1)S(1)} %shard_map.73) | data formatting | bytes 262144

commit v3 on v2

--- a/solution.py
+++ b/solution.py
@@ -12,7 +12,6 @@
 MESH = pl.DeviceIdType.MESH
 F32 = jnp.float32
 BF16 = jnp.bfloat16
-PIECES = 4
 
 
 def layer_kernel(
@@ -44,6 +43,7 @@
     tok_recv,
     wo_send,
     wo_recv,
+    wo_swap,
     kv_send,
     kv_recv,
     q_send,
@@ -125,30 +125,48 @@
             )
         return out
 
-    wo_rows = wo_buf.shape[1] // PIECES
-
-    class wo_piece:
-        def __init__(self, c):
-            self.rows = pl.ds(c * wo_rows, wo_rows)
-
-        @property
-        def at(self):
-            return self
-
-        def __getitem__(self, source):
-            return wo_buf.at[source, self.rows]
-
-    def wo_relay(c):
+    pieces = wo_send.shape[0]
+    wo_rows = wo_buf.shape[1] // pieces
+
+    def wo_at(source, c):
+        return wo_buf.at[source, pl.ds(pl.multiple_of(c * wo_rows, wo_rows), wo_rows)]
+
+    def start_all(copies):
+        for copy in copies:
+            copy.start()
+            wo_pending.append(copy)
+
+    def wo_send_to(source, c, slot, device):
+        return send(wo_at(source, c), wo_at(source, c), wo_send.at[c, slot], wo_recv.at[source, c], device)
+
+    def wo_far(c):
+        return [wo_send_to(t, c, i * lanes, (s, (pair_hi + i) % n_hi * lanes + pair_lo)) for i in range(1, n_hi)]
+
+    def wo_near(c, i=0):
+        source = (pair_hi + i) % n_hi * lanes + pair_lo
+        return [
+            wo_send_to(source, c, i * lanes + j, (s, pair_hi * lanes + (pair_lo + j) % lanes))
+            for j in range(1, lanes)
+        ]
+
+    def wo_wait(source, c):
+        pltpu.make_async_copy(wo_at(source, c), wo_at(source, c), wo_recv.at[source, c]).wait()
+
+    def wo_relay(c, across):
         for i in range(1, n_hi):
             source = (pair_hi + i) % n_hi * lanes + pair_lo
-            arrival(wo_piece(c), wo_recv.at[c], source)
-            for copy in relays(wo_piece(c), wo_send.at[c], wo_recv.at[c], i, source):
-                copy.start()
-                wo_pending.append(copy)
+            wo_wait(source, c)
+            if across:
+                for j in range(1, heads):
+                    device = (a * heads + (b + j) % heads, t)
+                    start_all(
+                        [send(wo_at(source, c), wo_at(source, c), wo_swap.at[i, j], wo_recv.at[source, c], device)]
+                    )
+            start_all(wo_near(c, i))
 
     def wo_arrival(source):
-        for c in range(PIECES):
-            arrival(wo_piece(c), wo_recv.at[c], source)
+        for c in range(pieces):
+            wo_wait(source, c)
 
     gain = gain_ref[...]
 
@@ -164,10 +182,10 @@
 
     loads[4].wait()
     wo_pending = []
-    for c in range(PIECES):
-        for copy in gather(wo_piece(c), wo_send.at[c], wo_recv.at[c]):
-            copy.start()
-            wo_pending.append(copy)
+    for c in [b] + list(range(heads, pieces)):
+        start_all(wo_far(c))
+    for c in range(pieces):
+        start_all(wo_near(c))
 
     @pl.when(has_next)
     def _():
@@ -227,10 +245,11 @@
 
     def kv_start(i, carry):
         for j in range(heads):
-            kv_copy(later - i, j).start()
+            kv_copy(i + 1, j).start()
         return carry
 
     lax.fori_loop(0, later, kv_start, 0)
+    wo_relay(b, True)
     kv_buf[a, mine, :] = kv_out[b]
     q_buf[mine, :] = q_out[b]
 
@@ -271,7 +290,7 @@
         kv_arrival(a, (b + j) % heads)
     total, kept = block(a, True, jnp.zeros((span, width), F32), jnp.zeros((span, 1), F32))
 
-    wo_relay(0)
+    wo_relay(heads, False)
 
     def absorb(i, carry):
         group = a - 1 - i
@@ -302,25 +321,27 @@
         copy.start()
     att_buf[t * heads + b] = att_out[b * n_tp + t]
 
-    wo_relay(1)
-    wo_relay(2)
-    for j in range(heads):
-        for i in range(n_tp):
-            if i or j:
-                arrival(att_buf, att_recv, (t + i) % n_tp * heads + (b + j) % heads)
+    for c in range(heads + 1, pieces):
+        wo_relay(c, False)
+    for j in range(1, heads):
+        wo_relay((b + j) % heads, False)
 
     def partial(source):
+        for h in range(heads):
+            if source is t:
+                continue
+            arrival(att_buf, att_recv, source * heads + h)
         parts = [att_buf[source * heads + h][:, HEAD_DIM:] for h in range(heads)]
         part = jnp.dot(jnp.concatenate(parts, axis=1), wo_buf[source], preferred_element_type=F32)
         return part.astype(BF16).astype(F32)
 
+    for j in range(1, heads):
+        arrival(att_buf, att_recv, t * heads + (b + j) % heads)
     mixed = partial(t)
     for j in range(1, lanes):
         source = pair_hi * lanes + (pair_lo + j) % lanes
         wo_arrival(source)
         mixed = mixed + partial(source)
-    for c in range(3, PIECES):
-        wo_relay(c)
     for i in range(1, n_hi):
         mixed = mixed + partial((pair_hi + i) % n_hi * lanes + pair_lo)
     for i in range(1, n_hi):
@@ -335,7 +356,7 @@
 
     def kv_done(i, carry):
         for j in range(heads):
-            kv_copy(later - i, j).wait_send()
+            kv_copy(i + 1, j).wait_send()
         return carry
 
     lax.fori_loop(0, later, kv_done, 0)
@@ -383,8 +404,9 @@
             dma((5,)),
             dma((n_tp,)),
             dma((n_tp,)),
-            dma((PIECES, n_tp)),
-            dma((PIECES, n_tp)),
+            dma((2 * heads, n_tp)),
+            dma((n_tp, 2 * heads)),
+            dma((n_tp // lanes, heads)),
             dma((groups, heads)),
             dma((n_sp,)),
             dma((heads,)),

time: 25.1 us -> 23.4 us (0.932)
  the two profiles are of different devices: /device:TPU:21 before, /device:TPU:25 now
where the time goes in v3:
time: 23.4 us; the launch traced here: 23.2 us
  Pallas kernels  22.5 us (96%)
  local copies, waits for them, and re-layouts  0.66 us (3%)
    pallas_call x1, Pallas kernels, per_device(): pl.pallas_call(functools.partial(layer_kernel, n_sp, n_tp, lanes), out_sh...  22.5 us
    unnamed x1, local copies, waits for them, and re-layouts  0.66 us

profile of v3, /device:TPU:25, one launch (start us, length us, event | category | flops | bytes accessed | tf_op | source)
XLA Modules:
  0.0 23.2 jit_solution(11849354970463740215)
XLA Ops:
  0.0 22.5 %shard_map.73 = bf16[32,2048]{1,0:T(8,128)(2,1)S(1)} custom-call(bf16[32,2048]{1,0:T(8,128)(2,1)} %tok_ref.1, f32[1,2048]{1,0:T(1,128)} %bitcast.1, bf16[2048,128]{1,0:T(8,128)(2,1)} %wq_ref.1, bf16[2048,128]{1,0:T(8,128)(2,1)} %wk_ref.1, bf16[2048,128]{1,0:T(8,128)(2,1)} %wv_ref.1, f32[2]{0:T(128)} %off_ref.1, bf16[128,2048]{1,0:T(8,128)(2,1)} %wout_ref.1), custom_call_target="tpu_custom_call" | custom-call | tf_op jit(solution)/shard_map/pallas_call | solution.py:378
  22.5 0.7 %copy.9 = bf16[32,2048]{1,0:T(8,128)(2,1)} copy(bf16[32,2048]{1,0:T(8,128)(2,1)S(1)} %shard_map.73) | data formatting | bytes 262144

commit v4 on v3

--- a/solution.py
+++ b/solution.py
@@ -202,6 +202,63 @@
         source = pair_hi * lanes + (pair_lo + j) % lanes
         arrival(tok_buf, tok_recv, source)
         norm(source)
+    for load in loads[1:4]:
+        load.wait()
+
+    chunk = lanes * piece
+    later = groups - 1 - a
+    kv_sends = []
+
+    def project(i):
+        span = pl.ds(pl.multiple_of((pair_hi + i) % n_hi * chunk, chunk), chunk)
+        projected = jnp.dot(normed[span, :], w_buf[...], preferred_element_type=F32).astype(BF16)
+        blank = jnp.zeros((chunk, HEAD_DIM), BF16)
+        for h in range(heads):
+            cols = slice(h * HEAD_DIM, (h + 1) * HEAD_DIM)
+            keys = projected[:, width:][:, cols]
+            vals = projected[:, 2 * width :][:, cols]
+            kv_out[h, span, :] = jnp.concatenate([keys, vals], axis=1)
+            q_out[h, span, :] = jnp.concatenate([projected[:, cols] * jnp.asarray(HEAD_DIM**-0.5, BF16), blank], axis=1)
+
+    def spans(i):
+        part = (pair_hi + i) % n_hi
+        here = pl.ds(pl.multiple_of(part * chunk, chunk), chunk)
+        there = pl.ds(pl.multiple_of(b * rows + part * chunk, chunk), chunk)
+        return part, here, there
+
+    def kv_copy(k, j, i):
+        h = (b + j) % heads
+        part, here, there = spans(i)
+        return send(
+            kv_out.at[h, here],
+            kv_buf.at[a, there],
+            kv_send.at[k, i * heads + j],
+            kv_recv.at[s, part],
+            ((a + k) * heads + h, t),
+        )
+
+    def send_chunks(i):
+        for j in range(1, heads):
+            h = (b + j) % heads
+            part, here, there = spans(i)
+            pair = [
+                send(q_out.at[h, here], q_buf.at[there], q_send.at[j, i], q_recv.at[b, part], (a * heads + h, t)),
+                kv_copy(0, j, i),
+            ]
+            for copy in pair:
+                copy.start()
+            kv_sends.extend(pair)
+
+        def kv_start(k, carry):
+            for j in range(heads):
+                kv_copy(k, j, i).start()
+            return carry
+
+        lax.fori_loop(1, later + 1, kv_start, 0)
+
+    project(0)
+    pl.semaphore_wait(pair_sem, heads - 1)
+    send_chunks(0)
     for i in range(1, n_hi):
         source = (pair_hi + i) % n_hi * lanes + pair_lo
         arrival(tok_buf, tok_recv, source)
@@ -209,54 +266,24 @@
             copy.start()
             pending.append(copy)
         norm(source)
-    pl.semaphore_wait(pair_sem, heads - 1)
     for i in range(1, n_hi):
         for j in range(1, lanes):
             source = (pair_hi + i) % n_hi * lanes + (pair_lo + j) % lanes
             arrival(tok_buf, tok_recv, source)
             norm(source)
-    for load in loads[1:4]:
-        load.wait()
-
-    projected = jnp.dot(normed[...], w_buf[...], preferred_element_type=F32).astype(BF16)
-    blank = jnp.zeros((rows, HEAD_DIM), BF16)
-    for h in range(heads):
-        cols = slice(h * HEAD_DIM, (h + 1) * HEAD_DIM)
-        keys = projected[:, width:][:, cols]
-        vals = projected[:, 2 * width :][:, cols]
-        kv_out[h] = jnp.concatenate([keys, vals], axis=1)
-        q_out[h] = jnp.concatenate([projected[:, cols] * jnp.asarray(HEAD_DIM**-0.5, BF16), blank], axis=1)
-
+    for i in range(1, n_hi):
+        project(i)
+        send_chunks(i)
     mine = pl.ds(pl.multiple_of(b * rows, rows), rows)
-    kv_sends = []
-    for j in range(1, heads):
-        h = (b + j) % heads
-        dest = (a * heads + h, t)
-        kv_sends.append(send(q_out.at[h], q_buf.at[mine], q_send.at[j], q_recv.at[b], dest))
-        kv_sends.append(send(kv_out.at[h], kv_buf.at[a, mine], kv_send.at[0, j], kv_recv.at[s], dest))
-    for copy in kv_sends:
-        copy.start()
-
-    def kv_copy(k, j):
-        h = (b + j) % heads
-        return send(kv_out.at[h], kv_buf.at[a, mine], kv_send.at[k, j], kv_recv.at[s], ((a + k) * heads + h, t))
-
-    later = groups - 1 - a
-
-    def kv_start(i, carry):
-        for j in range(heads):
-            kv_copy(i + 1, j).start()
-        return carry
-
-    lax.fori_loop(0, later, kv_start, 0)
     wo_relay(b, True)
     kv_buf[a, mine, :] = kv_out[b]
     q_buf[mine, :] = q_out[b]
 
     for j in range(1, heads):
         peer = (b + j) % heads
-        spot = pl.ds(pl.multiple_of(peer * rows, rows), rows)
-        pltpu.make_async_copy(q_buf.at[spot], q_buf.at[spot], q_recv.at[peer]).wait()
+        for part in range(n_hi):
+            spot = pl.ds(pl.multiple_of(peer * rows + part * chunk, chunk), chunk)
+            pltpu.make_async_copy(q_buf.at[spot], q_buf.at[spot], q_recv.at[peer, part]).wait()
 
     span = heads * rows
     offset = off_ref[b]
@@ -283,8 +310,9 @@
         return total, kept + suffix[:, :1] + log_keep[:, :1]
 
     def kv_arrival(group, peer):
-        spot = kv_buf.at[group, pl.ds(pl.multiple_of(peer * rows, rows), rows)]
-        pltpu.make_async_copy(spot, spot, kv_recv.at[group * heads + peer]).wait()
+        for part in range(n_hi):
+            spot = kv_buf.at[group, pl.ds(pl.multiple_of(peer * rows + part * chunk, chunk), chunk)]
+            pltpu.make_async_copy(spot, spot, kv_recv.at[group * heads + peer, part]).wait()
 
     for j in range(1, heads):
         kv_arrival(a, (b + j) % heads)
@@ -354,12 +382,13 @@
     for copy in pending + wo_pending + kv_sends + att_sends:
         copy.wait_send()
 
-    def kv_done(i, carry):
+    def kv_done(k, carry):
         for j in range(heads):
-            kv_copy(i + 1, j).wait_send()
+            for i in range(n_hi):
+                kv_copy(k, j, i).wait_send()
         return carry
 
-    lax.fori_loop(0, later, kv_done, 0)
+    lax.fori_loop(1, later + 1, kv_done, 0)
 
 
 def per_device(tokens, norm_gain, w_query, w_key, w_value, score_offset, w_out):
@@ -407,10 +436,10 @@
             dma((2 * heads, n_tp)),
             dma((n_tp, 2 * heads)),
             dma((n_tp // lanes, heads)),
-            dma((groups, heads)),
-            dma((n_sp,)),
-            dma((heads,)),
-            dma((heads,)),
+            dma((groups, heads * (n_tp // lanes))),
+            dma((n_sp, n_tp // lanes)),
+            dma((heads, n_tp // lanes)),
+            dma((heads, n_tp // lanes)),
             dma((heads * n_tp,)),
             dma((heads * n_tp,)),
         ],

time: 23.4 us -> 21.7 us (0.927)
  the two profiles are of different devices: /device:TPU:25 before, /device:TPU:0 now
where the time goes in v4:
time: 21.7 us; the launch traced here: 21.3 us
  Pallas kernels  20.6 us (95%)
  local copies, waits for them, and re-layouts  0.66 us (3%)
    pallas_call x1, Pallas kernels, per_device(): pl.pallas_call(functools.partial(layer_kernel, n_sp, n_tp, lanes), out_sh...  20.6 us
    unnamed x1, local copies, waits for them, and re-layouts  0.66 us

profile of v4, /device:TPU:0, one launch (start us, length us, event | category | flops | bytes accessed | tf_op | source)
XLA Modules:
  0.0 21.3 jit_solution(8510033811878867374)
XLA Ops:
  0.0 20.6 %shard_map.73 = bf16[32,2048]{1,0:T(8,128)(2,1)S(1)} custom-call(bf16[32,2048]{1,0:T(8,128)(2,1)} %tok_ref.1, f32[1,2048]{1,0:T(1,128)} %bitcast.1, bf16[2048,128]{1,0:T(8,128)(2,1)} %wq_ref.1, bf16[2048,128]{1,0:T(8,128)(2,1)} %wk_ref.1, bf16[2048,128]{1,0:T(8,128)(2,1)} %wv_ref.1, f32[2]{0:T(128)} %off_ref.1, bf16[128,2048]{1,0:T(8,128)(2,1)} %wout_ref.1), custom_call_target="tpu_custom_call" | custom-call | tf_op jit(solution)/shard_map/pallas_call | solution.py:407
  20.7 0.7 %copy.9 = bf16[32,2048]{1,0:T(8,128)(2,1)} copy(bf16[32,2048]{1,0:T(8,128)(2,1)S(1)} %shard_map.73) | data formatting | bytes 262144
